TPU v7x, 256 devices: a whole 4x4x8 slice. The times are simulated.
256 devices in a mesh: ep: 16 (over y, x), tp: 16 (over z, core).
Axes of the slice: x: 4, y: 4, z: 8, core: 2. Of those that a mesh axis runs over, the one named last changes fastest.
Arguments:
- tokens: bfloat16 [8192, 1024], P(('ep', 'tp')), may hold values from -6 to 6
- norm_gain: float32 [1024], replicated, may hold values from 0.5 to 1.5
- routing: int32 [8192, 2], P('ep'), may hold values from 0 to 31, as said below
- gate_share: float32 [8192, 2], P('ep'), may hold values from 0.5 to 1.5
- w_gate: bfloat16 [32, 1024, 256], P('ep', None, 'tp'), may hold values from -0.1875 to 0.1875
- w_up: bfloat16 [32, 1024, 256], P('ep', None, 'tp'), may hold values from -0.1875 to 0.1875
- w_down: bfloat16 [32, 256, 1024], P('ep', 'tp'), may hold values from -0.375 to 0.375
Outputs:
- mixed_out: bfloat16 [8192, 1024], P('ep', 'tp')
Inputs may be any that keep to these rules, and one draw needn't show every extreme that they name: `routing`: each row names two different experts whose ids lie in the same block of 8 consecutive ids. In each aligned block of 512 rows (the tokens of one index of ep) no expert is named by more than 64 rows, and some expert is named by exactly 64.
All inputs are finite; a program needn't handle non-finite values.
Results may differ from a plain program's by a relative error of at most 0.0015.
Values may be sent and summed in bfloat16 or wider, within the bound.
No kernel may reach another device: no remote copies, remote signals or barrier semaphores. Data moves between devices by JAX's collectives and lax.ppermute only.
A program may use at most 64 MiB of HBM per device.

v0:
```python
import jax
import jax.numpy as jnp
from jax import lax
from jax.sharding import PartitionSpec as P

epsilon = 1e-06


def in_order(parts, dim):
    shape = list(parts.shape[1:])
    shape[dim] *= parts.shape[0]
    return jnp.moveaxis(parts, 0, dim).reshape(shape)


def gather_together(arrays, axis, dims):
    flat = jnp.concatenate([a.reshape(-1) for a in arrays])
    lines, at, outs = (lax.all_gather(flat, axis), 0, [])
    for a, dim in zip(arrays, dims):
        parts = lines[:, at : at + a.size].reshape(-1, *a.shape)
        outs.append(in_order(parts, dim))
        at += a.size
    return tuple(outs)


def norm_rows(tokens, norm_gain):
    as_float = tokens.astype(jnp.float32)
    scaled = as_float * lax.rsqrt(jnp.mean(as_float * as_float, axis=-1, keepdims=True) + epsilon)
    return (scaled * norm_gain.astype(jnp.float32)).astype(jnp.bfloat16)


def fill_buffer(group, flat_target, slots, model_width):
    buffer = jnp.zeros((slots, model_width), jnp.bfloat16)
    return buffer.at[flat_target].set(jnp.repeat(group, 2, axis=0))


def body(tokens, norm_gain, routing, gate_share, w_gate, w_up, w_down):
    ep_size = lax.axis_size("ep")
    tp_size = lax.axis_size("tp")
    local_experts = w_gate.shape[0]
    experts = local_experts * ep_size
    group_rows = routing.shape[0]
    capacity = group_rows * 4 // experts
    model_width = tokens.shape[1]
    columns = model_width // tp_size
    normed = norm_rows(tokens, norm_gain)
    onehot = (routing[:, :, None] == jnp.arange(experts, dtype=jnp.int32)[None, None, :]).astype(
        jnp.int32
    )
    flat_hot = onehot.reshape(group_rows * 2, experts)
    ranking = jnp.cumsum(flat_hot, axis=0) - 1
    slot_pos = jnp.sum(ranking * flat_hot, axis=1).reshape(group_rows, 2)
    target = (routing * capacity + slot_pos).astype(jnp.int32)
    flat_target = target.reshape(-1)
    slice_len = capacity // tp_size
    tp_index = lax.axis_index("tp")
    group = lax.all_gather(normed, "tp", axis=0, tiled=True)
    buffer = fill_buffer(group, flat_target, experts * capacity, model_width)
    shaped = buffer.reshape(ep_size, local_experts, capacity, model_width)
    mine = lax.dynamic_slice_in_dim(shaped, tp_index * slice_len, slice_len, 2)
    mine = mine.reshape(ep_size, local_experts * slice_len, model_width)
    landed = lax.all_to_all(mine, "ep", split_axis=0, concat_axis=0, tiled=True)
    landed = landed.reshape(ep_size, local_experts, slice_len, model_width).transpose(1, 0, 2, 3)
    landed = landed.reshape(local_experts, ep_size * slice_len, model_width)
    full_gate, full_up, full_down = gather_together((w_gate, w_up, w_down), "tp", (2, 2, 1))
    gate_sum = jnp.einsum("erd,edh->erh", landed, full_gate, preferred_element_type=jnp.float32)
    up_sum = jnp.einsum("erd,edh->erh", landed, full_up, preferred_element_type=jnp.float32)
    hidden = (jax.nn.silu(gate_sum) * up_sum).astype(jnp.bfloat16)
    produced = jnp.einsum(
        "erh,ehd->erd", hidden, full_down, preferred_element_type=jnp.float32
    ).astype(jnp.bfloat16)
    produced = produced.reshape(local_experts, ep_size, slice_len, model_width)
    blocks = lax.all_to_all(produced, "tp", split_axis=3, concat_axis=2, tiled=True)
    leaving = blocks.transpose(1, 0, 2, 3).reshape(ep_size, local_experts * capacity, columns)
    returned = lax.all_to_all(leaving, "ep", split_axis=0, concat_axis=0, tiled=True).reshape(
        experts * capacity, columns
    )
    picked_out = returned[target]
    mixed_out = jnp.sum(gate_share[:, :, None] * picked_out.astype(jnp.float32), axis=1)
    return mixed_out.astype(jnp.bfloat16)


def solution(mesh):
    return jax.shard_map(
        body,
        mesh=mesh,
        in_specs=(
            P(("ep", "tp"), None),
            P(),
            P("ep", None),
            P("ep", None),
            P("ep", None, "tp"),
            P("ep", None, "tp"),
            P("ep", "tp", None),
        ),
        out_specs=P("ep", "tp"),
        check_vma=False,
    )
```

profile of v0, /device:TPU:1, one launch (start us, length us, event | category | flops | bytes accessed | tf_op | source)
XLA Modules:
  0.0 184.5 jit_solution(3607458096180063243)
XLA Ops:
  7.5 1.6 fusion.6
  14.2 9.0 %reduce-window.6 = s32[32,8,128]{2,1,0:T(8,128)S(1)} reduce-window(s32[32,8,128]{2,1,0:T(8,128)S(1)} %fusion.14, s32[]{:T(128)} %constant.13.clone.1), window={size=1x1x128 pad=0_0x0_0x127_0}, to_apply=%region_0.0 | reduce-window | flops 4161536 | bytes 262148 | tf_op jit(solution)/shard_map/reduce-window
  24.4 27.6 %all-gather.4.cloned.1.call-done = bf16[512,1024]{1,0:T(8,128)(2,1)} async-done(((bf16[32,1024]{1,0:T(8,128)(2,1)}), bf16[512,1024]{1,0:T(8,128)(2,1)}) %all-gather.4.cloned.1.call-update) | async-done | bytes 1048592 | tf_op jit(solution)/shard_map/all_gather | solution.py:56
  52.0 2.3 %broadcast_in_dim.7 = bf16[512,2,1024]{2,1,0:T(2,128)(2,1)S(1)} broadcast(bf16[512,1024]{1,0:T(8,128)(2,1)} %all-gather.4.cloned.1.call-done), dimensions={0,2} | broadcast | bytes 3145728 | tf_op jit(solution)/shard_map/broadcast_in_dim | solution.py:33
  54.3 2.3 %reshape.147 = bf16[1024,1024]{1,0:T(8,128)(2,1)} reshape(bf16[512,2,1024]{2,1,0:T(2,128)(2,1)S(1)} %broadcast_in_dim.7) | data formatting | bytes 4194304 | tf_op jit(solution)/shard_map/reshape | solution.py:33
  56.6 8.6 %scatter_custom_fusion = bf16[2048,1024]{1,0:T(8,128)(2,1)} fusion(s32[1024]{0:T(1024)S(1)} %bitcast.70, bf16[1024,1024]{1,0:T(8,128)(2,1)} %reshape.147, bf16[]{:T(256)} %constant.11.clone.1), kind=kCustom, calls=%fused_computation.2 | custom fusion | bytes 4194816 | tf_op jit(solution)/shard_map/scatter | solution.py:33
  65.2 1.2 constant_dynamic-slice_fusion
  66.7 14.5 %all_to_all.28 = bf16[16,8,1024]{2,1,0:T(8,128)(2,1)S(1)} all-to-all(bf16[16,8,1024]{2,1,0:T(8,128)(2,1)S(1)} %copy.93), channel_id=1, replica_groups=mesh['ep'=16,'tp'=16] {'ep'}, dimensions={0} | all-to-all | bytes 524288 | tf_op jit(solution)/shard_map/all_to_all | solution.py:61
  81.7 11.3 %all-gather.6.cloned.1.call-done = bf16[1572864]{0:T(1024)(128)(2,1)} async-done(((bf16[98304]{0:T(1024)(128)(2,1)}), bf16[1572864]{0:T(1024)(128)(2,1)}) %all-gather.6.cloned.1.call-update) | async-done | bytes 3145744 | tf_op jit(solution)/shard_map/all_gather | solution.py:17
  93.0 2.8 %reshape.151 = bf16[16,98304]{1,0:T(8,128)(2,1)S(1)} reshape(bf16[1572864]{0:T(1024)(128)(2,1)} %all-gather.6.cloned.1.call-done) | data formatting | bytes 6291456 | tf_op jit(solution)/shard_map/all_gather | solution.py:17
  95.7 1.8 fusion.17
  97.6 9.6 %reshape.126 = bf16[16,2,1024,16]{3,2,1,0:T(8,128)(2,1)} reshape(bf16[16,32768]{1,0:T(8,128)(2,1)} %get-tuple-element.7) | data formatting | bytes 2097152 | tf_op jit(solution)/shard_map/reshape | solution.py:19
  107.2 6.8 %copy.98 = bf16[2,1024,16,16]{1,3,2,0:T(8,128)(2,1)S(1)} copy(bf16[2,1024,16,16]{3,1,0,2:T(8,128)(2,1)} %bitcast.51) | data formatting | bytes 2097152 | tf_op jit(solution)/shard_map/transpose | solution.py:12
  114.0 8.9 %reshape.128 = bf16[16,2,1024,16]{3,2,1,0:T(8,128)(2,1)} reshape(bf16[16,32768]{1,0:T(8,128)(2,1)S(1)} %copy-done) | data formatting | bytes 2097152 | tf_op jit(solution)/shard_map/reshape | solution.py:19
  122.9 6.8 %copy.100 = bf16[2,1024,16,16]{1,3,2,0:T(8,128)(2,1)S(1)} copy(bf16[2,1024,16,16]{3,1,0,2:T(8,128)(2,1)} %bitcast.52) | data formatting | bytes 2097152 | tf_op jit(solution)/shard_map/transpose | solution.py:12
  131.7 1.4 copy.103
  133.1 2.1 %reshape.157 = bf16[16,2,4096]{2,1,0:T(2,128)(2,1)S(1)} reshape(bf16[1024,2,4,16]{3,2,1,0:T(4,128)(2,1)S(1)} %bitcast.55) | data formatting | bytes 524288
  135.3 16.0 %all_to_all.29 = bf16[16,2,4096]{2,1,0:T(2,128)(2,1)S(1)} all-to-all(bf16[16,2,4096]{2,1,0:T(2,128)(2,1)S(1)} %reshape.157), channel_id=1, replica_groups=mesh['ep'=16,'tp'=16] {'tp'}, dimensions={0} | all-to-all | bytes 524288 | tf_op jit(solution)/shard_map/all_to_all | solution.py:72
  151.3 1.4 reshape.158
  152.7 1.6 copy.113
  155.4 6.5 %all-to-all-start.2 = ((bf16[16,128,64]{1,2,0:T(8,128)(2,1)}), bf16[16,128,64]{1,2,0:T(8,128)(2,1)S(1)}, u32[]{:S(2)}, u32[]{:S(2)}) async-start(bf16[16,128,64]{1,2,0:T(8,128)(2,1)} %copy.106), calls=%async_computation.2 | async-start | bytes 524288 | tf_op jit(solution)/shard_map/all_to_all | solution.py:74
  162.5 8.0 %all-to-all-done.2 = bf16[16,128,64]{1,2,0:T(8,128)(2,1)S(1)} async-done(((bf16[16,128,64]{1,2,0:T(8,128)(2,1)}), bf16[16,128,64]{1,2,0:T(8,128)(2,1)S(1)}, u32[]{:S(2)}, u32[]{:S(2)}) %all-to-all-start.2) | async-done | bytes 262176 | tf_op jit(solution)/shard_map/all_to_all | solution.py:74
  170.8 3.2 %gather_fusion = bf16[1024,64]{1,0:T(8,128)(2,1)S(1)} fusion(bf16[2048,64]{1,0:T(8,128)(2,1)S(1)} %bitcast.53, s32[1024]{0:T(1024)S(1)} %broadcast_clamp_fusion), kind=kCustom, calls=%fused_computation | custom fusion | bytes 266240 | tf_op jit(solution)/shard_map/gather | solution.py:77
  174.1 2.8 %fusion.3 = bf16[512,64]{1,0:T(8,128)(2,1)S(1)} fusion(bf16[512,2,64]{2,1,0:T(2,128)(2,1)S(1)} %bitcast.63, f32[512,2]{1,0:T(8,128)S(1)} %copy.85), kind=kLoop, calls=%fused_computation.8 | loop fusion | flops 163840 | bytes 200704 | tf_op jit(solution)/shard_map/reduce_sum | solution.py:78
  (54 shorter events, 12.4 us)
Async XLA Ops:
  6.5 7.1 %copy-start.2 = (s32[512,2]{0,1:T(2,128)S(1)}, s32[512,2]{0,1:T(2,128)}, u32[]{:S(2)}) copy-start(s32[512,2]{0,1:T(2,128)} %param.9) | copy-start | bytes 12292
  6.5 45.5 %all-gather.4.cloned.1.call-start = ((), (), s32[]{:S(2)}) async-start(), calls=%async_computation.3 | async-start | bytes 1114112 | tf_op jit(solution)/shard_map/all_gather | solution.py:56
  9.1 83.9 %all-gather.6.cloned.1.call-start = ((), (), s32[]{:S(2)}) async-start(), calls=%async_computation.4 | async-start | bytes 3342336 | tf_op jit(solution)/shard_map/all_gather | solution.py:17
  107.2 6.8 %copy-start = (bf16[16,32768]{1,0:T(8,128)(2,1)S(1)}, bf16[16,32768]{1,0:T(8,128)(2,1)}, u32[]{:S(2)}) copy-start(bf16[16,32768]{1,0:T(8,128)(2,1)} %get-tuple-element.9) | copy-start | bytes 3145732
  122.9 6.8 %copy-start.1 = (bf16[16,32768]{1,0:T(8,128)(2,1)S(1)}, bf16[16,32768]{1,0:T(8,128)(2,1)}, u32[]{:S(2)}) copy-start(bf16[16,32768]{1,0:T(8,128)(2,1)} %get-tuple-element.8) | copy-start | bytes 3145732
  151.3 11.0 %copy-start.3 = (f32[512,2]{0,1:T(2,128)S(1)}, f32[512,2]{0,1:T(2,128)}, u32[]{:S(2)}) copy-start(f32[512,2]{0,1:T(2,128)} %param.10) | copy-start | bytes 12292
  155.4 15.1 %all-to-all-start.2 = ((bf16[16,128,64]{1,2,0:T(8,128)(2,1)}), bf16[16,128,64]{1,2,0:T(8,128)(2,1)S(1)}, u32[]{:S(2)}, u32[]{:S(2)}) async-start(bf16[16,128,64]{1,2,0:T(8,128)(2,1)} %copy.106), calls=%async_computation.2 | async-start | bytes 524288 | tf_op jit(solution)/shard_map/all_to_all | solution.py:74
Sparse Core Ops, SparseCore 0:
  9.2 42.7 all-gather.3
  53.8 39.0 all-gather.5
where the time goes:
time: 185 us; the launch traced here: 184 us
  local copies, waits for them, and re-layouts  70.2 us (38%)
  waiting for transfers between devices  47 us (25%)
  blocking collectives  30.5 us (16%)
  other arithmetic  15.3 us (8%)
  between operations  13.7 us (7%)
  starting transfers between devices  6.57 us (4%)
    all_gather x1, waiting for transfers between devices, body(): group = lax.all_gather(normed, 'tp', axis=0, tiled=True)  27.6 us
    reshape x2, local copies, waits for them, and re-layouts, gather_together(): parts = lines[:, at:at + a.size].reshape(-1, *a.shape)  18.6 us
    all_to_all x1, blocking collectives, body(): lax.all_to_all(produced, 'tp', split_axis=3, concat_axis=2, tiled=True)  16 us
    all_to_all x1, blocking collectives, body(): landed = lax.all_to_all(mine, 'ep', split_axis=0, concat_axis=0, tiled=True)  14.5 us
    transpose x3, local copies, waits for them, and re-layouts, in_order(): return jnp.moveaxis(parts, 0, dim).reshape(shape)  13.7 us
    all_gather x1, waiting for transfers between devices, gather_together(): lines, at, outs = (lax.all_gather(flat, axis), 0, [])  11.3 us
    another operation x2, other arithmetic  9.04 us
    scatter x1, local copies, waits for them, and re-layouts, fill_buffer(): return buffer.at[flat_target].set(jnp.repeat(group, 2, axis=0))  8.55 us
  transfers between devices with their start and end apart: 3, of which 3 were waited for; matrix products, arithmetic and copies ran while one was open for 17% of the time, Pallas kernels for 0%

commit v1 on v0

--- a/solution.py
+++ b/solution.py
@@ -69,7 +69,24 @@
         "erh,ehd->erd", hidden, full_down, preferred_element_type=jnp.float32
     ).astype(jnp.bfloat16)
     produced = produced.reshape(local_experts, ep_size, slice_len, model_width)
-    blocks = lax.all_to_all(produced, "tp", split_axis=3, concat_axis=2, tiled=True)
+    small = lax.axis_size("tp")
+    z1 = lax.axis_index("tp")
+    extra, prior = (small, z1)
+    before = produced.shape[3] // extra
+    odd = list(produced.shape)
+    odd[3] = before
+    finding = odd[2]
+    odd[2] = finding * extra
+    blocks = jnp.zeros(odd, produced.dtype)
+    j = 0
+    while j < extra:
+        step_out = lax.dynamic_slice_in_dim(produced, (prior ^ j) * before, before, axis=3)
+        if j:
+            step_out = lax.ppermute(
+                step_out, axis_name="tp", perm=[(it, it ^ j) for it in range(extra)]
+            )
+        blocks = lax.dynamic_update_slice_in_dim(blocks, step_out, (prior ^ j) * finding, axis=2)
+        j += 1
     leaving = blocks.transpose(1, 0, 2, 3).reshape(ep_size, local_experts * capacity, columns)
     returned = lax.all_to_all(leaving, "ep", split_axis=0, concat_axis=0, tiled=True).reshape(
         experts * capacity, columns

time: 185 us -> 2780 us (15.03)
  local copies, waits for them, and re-layouts: 70.2 us -> 2650 us
  starting transfers between devices: 6.57 us -> 39.5 us
  blocking collectives: 30.5 us -> 0 us
    dynamic_update_slice x0 -> x16, local copies, waits for them, and re-layouts: none -> 2570 us  [body(): lax.dynamic_update_slice_in_dim(blocks, step_out, (prior ^ j) * finding,...]
    all_to_all x2 -> x0, blocking collectives: 30.5 us -> none  [the longest x1 16 us: body(): lax.all_to_all(produced, 'tp', split_axis=3, concat_axis=2, tiled=True)]
  transfers between devices with their start and end apart: 3 -> 19, of which waited for: 3 -> 4; matrix products, arithmetic and copies ran while one was open for 17% -> 88% of each run, Pallas kernels for 0% -> 0%
where the time goes in v1:
time: 2780 us; the launch traced here: 2770 us
  local copies, waits for them, and re-layouts  2650 us (95%)
  waiting for transfers between devices  53.4 us (2%)
  starting transfers between devices  39.5 us (1%)
    dynamic_update_slice x16, local copies, waits for them, and re-layouts, body(): lax.dynamic_update_slice_in_dim(blocks, step_out, (prior ^ j) * finding,...  2570 us
  transfers between devices with their start and end apart: 19, of which 4 were waited for; matrix products, arithmetic and copies ran while one was open for 88% of the time, Pallas kernels for 0%

profile of v1, /device:TPU:1, one launch (start us, length us, event | category | flops | bytes accessed | tf_op | source)
XLA Modules:
  0.0 2771.7 jit_solution(14235895379025559745)
XLA Ops:
  14.9 9.0 reduce-window.6
  25.1 26.9 all-gather.4.cloned.1.call-done
  56.6 8.6 scatter_custom_fusion
  74.2 8.1 all-to-all-done
  82.7 10.3 all-gather.6.cloned.1.call-done
  97.6 9.6 reshape.126
  114.0 8.9 reshape.128
  159.3 169.5 %dynamic_update_slice.48 = bf16[2,16,64,64]{2,0,3,1:T(2,128)(2,1)S(1)} dynamic-update-slice(bf16[2,16,64,64]{2,0,3,1:T(2,128)(2,1)S(1)} %broadcast_in_dim.8, bf16[2,16,4,64]{2,0,3,1:T(2,128)(2,1)S(1)} %copy.116, s32[]{:T(128)} %constant.28.clone.1, s32[]{:T(128)} %constant.28.clone.1, s32[]{:T(128)S(6)} %select_n.111, s32[]{:T(128)} %constant.28.clone.1) | dynamic-update-slice | bytes 32772 | tf_op jit(solution)/shard_map/dynamic_update_slice | solution.py:88
  329.3 31.8 %dynamic_update_slice.49 = bf16[2,16,64,64]{2,0,3,1:T(2,128)(2,1)S(1)} dynamic-update-slice(bf16[2,16,64,64]{2,0,3,1:T(2,128)(2,1)S(1)} %dynamic_update_slice.48, bf16[2,16,4,64]{2,0,3,1:T(2,128)(2,1)S(1)} %copy.117, s32[]{:T(128)} %constant.28.clone.1, s32[]{:T(128)} %constant.28.clone.1, s32[]{:T(128)S(6)} %select_n.114, s32[]{:T(128)} %constant.28.clone.1) | dynamic-update-slice | bytes 32772 | tf_op jit(solution)/shard_map/dynamic_update_slice | solution.py:88
  361.6 169.5 %dynamic_update_slice.50 = bf16[2,16,64,64]{2,0,3,1:T(2,128)(2,1)S(1)} dynamic-update-slice(bf16[2,16,64,64]{2,0,3,1:T(2,128)(2,1)S(1)} %dynamic_update_slice.49, bf16[2,16,4,64]{2,0,3,1:T(2,128)(2,1)S(1)} %copy.118, s32[]{:T(128)} %constant.28.clone.1, s32[]{:T(128)} %constant.28.clone.1, s32[]{:T(128)S(6)} %select_n.116, s32[]{:T(128)} %constant.28.clone.1) | dynamic-update-slice | bytes 32772 | tf_op jit(solution)/shard_map/dynamic_update_slice | solution.py:88
  531.7 169.5 %dynamic_update_slice.51 = bf16[2,16,64,64]{2,0,3,1:T(2,128)(2,1)S(1)} dynamic-update-slice(bf16[2,16,64,64]{2,0,3,1:T(2,128)(2,1)S(1)} %dynamic_update_slice.50, bf16[2,16,4,64]{2,0,3,1:T(2,128)(2,1)S(1)} %copy.119, s32[]{:T(128)} %constant.28.clone.1, s32[]{:T(128)} %constant.28.clone.1, s32[]{:T(128)S(6)} %select_n.118, s32[]{:T(128)} %constant.28.clone.1) | dynamic-update-slice | bytes 32772 | tf_op jit(solution)/shard_map/dynamic_update_slice | solution.py:88
  701.7 169.5 %dynamic_update_slice.52 = bf16[2,16,64,64]{2,0,3,1:T(2,128)(2,1)S(1)} dynamic-update-slice(bf16[2,16,64,64]{2,0,3,1:T(2,128)(2,1)S(1)} %dynamic_update_slice.51, bf16[2,16,4,64]{2,0,3,1:T(2,128)(2,1)S(1)} %copy.120, s32[]{:T(128)} %constant.28.clone.1, s32[]{:T(128)} %constant.28.clone.1, s32[]{:T(128)S(6)} %select_n.120, s32[]{:T(128)} %constant.28.clone.1) | dynamic-update-slice | bytes 32772 | tf_op jit(solution)/shard_map/dynamic_update_slice | solution.py:88
  871.7 169.5 %dynamic_update_slice.53 = bf16[2,16,64,64]{2,0,3,1:T(2,128)(2,1)S(1)} dynamic-update-slice(bf16[2,16,64,64]{2,0,3,1:T(2,128)(2,1)S(1)} %dynamic_update_slice.52, bf16[2,16,4,64]{2,0,3,1:T(2,128)(2,1)S(1)} %copy.121, s32[]{:T(128)} %constant.28.clone.1, s32[]{:T(128)} %constant.28.clone.1, s32[]{:T(128)S(6)} %select_n.122, s32[]{:T(128)} %constant.28.clone.1) | dynamic-update-slice | bytes 32772 | tf_op jit(solution)/shard_map/dynamic_update_slice | solution.py:88
  1041.7 169.5 %dynamic_update_slice.54 = bf16[2,16,64,64]{2,0,3,1:T(2,128)(2,1)S(1)} dynamic-update-slice(bf16[2,16,64,64]{2,0,3,1:T(2,128)(2,1)S(1)} %dynamic_update_slice.53, bf16[2,16,4,64]{2,0,3,1:T(2,128)(2,1)S(1)} %copy.122, s32[]{:T(128)} %constant.28.clone.1, s32[]{:T(128)} %constant.28.clone.1, s32[]{:T(128)S(6)} %select_n.124, s32[]{:T(128)} %constant.28.clone.1) | dynamic-update-slice | bytes 32772 | tf_op jit(solution)/shard_map/dynamic_update_slice | solution.py:88
  1211.7 169.5 %dynamic_update_slice.55 = bf16[2,16,64,64]{2,0,3,1:T(2,128)(2,1)S(1)} dynamic-update-slice(bf16[2,16,64,64]{2,0,3,1:T(2,128)(2,1)S(1)} %dynamic_update_slice.54, bf16[2,16,4,64]{2,0,3,1:T(2,128)(2,1)S(1)} %copy.123, s32[]{:T(128)} %constant.28.clone.1, s32[]{:T(128)} %constant.28.clone.1, s32[]{:T(128)S(6)} %select_n.126, s32[]{:T(128)} %constant.28.clone.1) | dynamic-update-slice | bytes 32772 | tf_op jit(solution)/shard_map/dynamic_update_slice | solution.py:88
  1381.8 169.7 %dynamic_update_slice.56 = bf16[2,16,64,64]{2,0,3,1:T(2,128)(2,1)S(1)} dynamic-update-slice(bf16[2,16,64,64]{2,0,3,1:T(2,128)(2,1)S(1)} %dynamic_update_slice.55, bf16[2,16,4,64]{2,0,3,1:T(2,128)(2,1)S(1)} %copy.124, s32[]{:T(128)} %constant.28.clone.1, s32[]{:T(128)} %constant.28.clone.1, s32[]{:T(128)S(6)} %select_n.128, s32[]{:T(128)} %constant.28.clone.1) | dynamic-update-slice | bytes 32772 | tf_op jit(solution)/shard_map/dynamic_update_slice | solution.py:88
  1551.9 169.5 %dynamic_update_slice.57 = bf16[2,16,64,64]{2,0,3,1:T(2,128)(2,1)S(1)} dynamic-update-slice(bf16[2,16,64,64]{2,0,3,1:T(2,128)(2,1)S(1)} %dynamic_update_slice.56, bf16[2,16,4,64]{2,0,3,1:T(2,128)(2,1)S(1)} %copy.125, s32[]{:T(128)} %constant.28.clone.1, s32[]{:T(128)} %constant.28.clone.1, s32[]{:T(128)S(6)} %select_n.130, s32[]{:T(128)} %constant.28.clone.1) | dynamic-update-slice | bytes 32772 | tf_op jit(solution)/shard_map/dynamic_update_slice | solution.py:88
  1722.0 169.5 %dynamic_update_slice.58 = bf16[2,16,64,64]{2,0,3,1:T(2,128)(2,1)S(1)} dynamic-update-slice(bf16[2,16,64,64]{2,0,3,1:T(2,128)(2,1)S(1)} %dynamic_update_slice.57, bf16[2,16,4,64]{2,0,3,1:T(2,128)(2,1)S(1)} %copy.126, s32[]{:T(128)} %constant.28.clone.1, s32[]{:T(128)} %constant.28.clone.1, s32[]{:T(128)S(6)} %select_n.132, s32[]{:T(128)} %constant.28.clone.1) | dynamic-update-slice | bytes 32772 | tf_op jit(solution)/shard_map/dynamic_update_slice | solution.py:88
  1892.0 169.5 %dynamic_update_slice.59 = bf16[2,16,64,64]{2,0,3,1:T(2,128)(2,1)S(1)} dynamic-update-slice(bf16[2,16,64,64]{2,0,3,1:T(2,128)(2,1)S(1)} %dynamic_update_slice.58, bf16[2,16,4,64]{2,0,3,1:T(2,128)(2,1)S(1)} %copy.127, s32[]{:T(128)} %constant.28.clone.1, s32[]{:T(128)} %constant.28.clone.1, s32[]{:T(128)S(6)} %select_n.134, s32[]{:T(128)} %constant.28.clone.1) | dynamic-update-slice | bytes 32772 | tf_op jit(solution)/shard_map/dynamic_update_slice | solution.py:88
  2062.0 169.5 %dynamic_update_slice.60 = bf16[2,16,64,64]{2,0,3,1:T(2,128)(2,1)S(1)} dynamic-update-slice(bf16[2,16,64,64]{2,0,3,1:T(2,128)(2,1)S(1)} %dynamic_update_slice.59, bf16[2,16,4,64]{2,0,3,1:T(2,128)(2,1)S(1)} %copy.128, s32[]{:T(128)} %constant.28.clone.1, s32[]{:T(128)} %constant.28.clone.1, s32[]{:T(128)S(6)} %select_n.136, s32[]{:T(128)} %constant.28.clone.1) | dynamic-update-slice | bytes 32772 | tf_op jit(solution)/shard_map/dynamic_update_slice | solution.py:88
  2232.1 169.5 %dynamic_update_slice.61 = bf16[2,16,64,64]{2,0,3,1:T(2,128)(2,1)S(1)} dynamic-update-slice(bf16[2,16,64,64]{2,0,3,1:T(2,128)(2,1)S(1)} %dynamic_update_slice.60, bf16[2,16,4,64]{2,0,3,1:T(2,128)(2,1)S(1)} %copy.129, s32[]{:T(128)} %constant.28.clone.1, s32[]{:T(128)} %constant.28.clone.1, s32[]{:T(128)S(6)} %select_n.138, s32[]{:T(128)} %constant.28.clone.1) | dynamic-update-slice | bytes 32772 | tf_op jit(solution)/shard_map/dynamic_update_slice | solution.py:88
  2402.1 169.5 %dynamic_update_slice.62 = bf16[2,16,64,64]{2,0,3,1:T(2,128)(2,1)S(1)} dynamic-update-slice(bf16[2,16,64,64]{2,0,3,1:T(2,128)(2,1)S(1)} %dynamic_update_slice.61, bf16[2,16,4,64]{2,0,3,1:T(2,128)(2,1)S(1)} %copy.130, s32[]{:T(128)} %constant.28.clone.1, s32[]{:T(128)} %constant.28.clone.1, s32[]{:T(128)S(6)} %select_n.140, s32[]{:T(128)} %constant.28.clone.1) | dynamic-update-slice | bytes 32772 | tf_op jit(solution)/shard_map/dynamic_update_slice | solution.py:88
  2572.1 169.5 %dynamic_update_slice.63 = bf16[2,16,64,64]{2,0,3,1:T(2,128)(2,1)S(1)} dynamic-update-slice(bf16[2,16,64,64]{2,0,3,1:T(2,128)(2,1)S(1)} %dynamic_update_slice.62, bf16[2,16,4,64]{2,0,3,1:T(2,128)(2,1)S(1)} %copy.131, s32[]{:T(128)} %constant.28.clone.1, s32[]{:T(128)} %constant.28.clone.1, s32[]{:T(128)S(6)} %select_n.142, s32[]{:T(128)} %constant.28.clone.1) | dynamic-update-slice | bytes 32772 | tf_op jit(solution)/shard_map/dynamic_update_slice | solution.py:88
  2749.6 8.0 all-to-all-done.1
  (114 shorter events, 93.4 us)
Async XLA Ops:
  6.5 18.2 copy-start.2
  6.5 45.5 %all-gather.4.cloned.1.call-start = ((), (), s32[]{:S(2)}) async-start(), calls=%async_computation.2 | async-start | bytes 1114112 | tf_op jit(solution)/shard_map/all_gather | solution.py:56
  9.1 83.9 %all-gather.6.cloned.1.call-start = ((), (), s32[]{:S(2)}) async-start(), calls=%async_computation.3 | async-start | bytes 3342336 | tf_op jit(solution)/shard_map/all_gather | solution.py:17
  67.4 14.9 all-to-all-start
  107.2 6.8 copy-start
  122.9 6.8 copy-start.1
  132.2 5.0 collective-permute-start
  132.6 7.1 collective-permute-start.1
  133.4 7.4 collective-permute-start.2
  134.4 9.2 collective-permute-start.3
  135.7 10.7 collective-permute-start.4
  137.1 10.0 collective-permute-start.5
  139.7 11.5 collective-permute-start.6
  140.8 10.7 collective-permute-start.7
  143.6 11.4 collective-permute-start.8
  146.3 10.0 collective-permute-start.9
  147.1 1744.4 %collective-permute-start.10 = (bf16[2,16,4,64]{3,2,1,0:T(4,128)(2,1)S(1)}, bf16[2,16,4,64]{3,2,1,0:T(4,128)(2,1)S(1)}, u32[]{:S(2)}, u32[]{:S(2)}) collective-permute-start(bf16[2,16,4,64]{3,2,1,0:T(4,128)(2,1)S(1)} %get-tuple-element.14), channel_id=1, source_target_pairs={{0,11},{1,10},{2,9},{3,8},{4,15},{5,14},{6,13},{7,12},{8,3},{9,2},... | collective-permute-start | bytes 49160 | tf_op jit(solution)/shard_map/ppermute | solution.py:85
  151.2 1910.3 %collective-permute-start.11 = (bf16[2,16,4,64]{3,2,1,0:T(4,128)(2,1)S(1)}, bf16[2,16,4,64]{3,2,1,0:T(4,128)(2,1)S(1)}, u32[]{:S(2)}, u32[]{:S(2)}) collective-permute-start(bf16[2,16,4,64]{3,2,1,0:T(4,128)(2,1)S(1)} %get-tuple-element.13), channel_id=1, source_target_pairs={{0,12},{1,13},{2,14},{3,15},{4,8},{5,9},{6,10},{7,11},{8,4},{9,5},... | collective-permute-start | bytes 49160 | tf_op jit(solution)/shard_map/ppermute | solution.py:85
  151.5 2080.1 %collective-permute-start.12 = (bf16[2,16,4,64]{3,2,1,0:T(4,128)(2,1)S(1)}, bf16[2,16,4,64]{3,2,1,0:T(4,128)(2,1)S(1)}, u32[]{:S(2)}, u32[]{:S(2)}) collective-permute-start(bf16[2,16,4,64]{3,2,1,0:T(4,128)(2,1)S(1)} %get-tuple-element.12), channel_id=1, source_target_pairs={{0,13},{1,12},{2,15},{3,14},{4,9},{5,8},{6,11},{7,10},{8,5},{9,4},... | collective-permute-start | bytes 49160 | tf_op jit(solution)/shard_map/ppermute | solution.py:85
  155.0 2246.6 %collective-permute-start.13 = (bf16[2,16,4,64]{3,2,1,0:T(4,128)(2,1)S(1)}, bf16[2,16,4,64]{3,2,1,0:T(4,128)(2,1)S(1)}, u32[]{:S(2)}, u32[]{:S(2)}) collective-permute-start(bf16[2,16,4,64]{3,2,1,0:T(4,128)(2,1)S(1)} %get-tuple-element.11), channel_id=1, source_target_pairs={{0,14},{1,15},{2,12},{3,13},{4,10},{5,11},{6,8},{7,9},{8,6},{9,7},... | collective-permute-start | bytes 49160 | tf_op jit(solution)/shard_map/ppermute | solution.py:85
  156.4 2415.2 %collective-permute-start.14 = (bf16[2,16,4,64]{3,2,1,0:T(4,128)(2,1)S(1)}, bf16[2,16,4,64]{3,2,1,0:T(4,128)(2,1)S(1)}, u32[]{:S(2)}, u32[]{:S(2)}) collective-permute-start(bf16[2,16,4,64]{3,2,1,0:T(4,128)(2,1)S(1)} %get-tuple-element.10), channel_id=1, source_target_pairs={{0,15},{1,14},{2,13},{3,12},{4,11},{5,10},{6,9},{7,8},{8,7},{9,6},... | collective-permute-start | bytes 49160 | tf_op jit(solution)/shard_map/ppermute | solution.py:85
  2061.5 687.9 %copy-start.3 = (f32[512,2]{0,1:T(2,128)S(1)}, f32[512,2]{0,1:T(2,128)}, u32[]{:S(2)}) copy-start(f32[512,2]{0,1:T(2,128)} %param.10) | copy-start | bytes 12292
  2742.6 15.0 all-to-all-start.1
Sparse Core Ops, SparseCore 0:
  9.2 42.7 all-gather.3
  53.8 39.1 all-gather.5
